TPU v7x, 256 devices: a whole 4x4x8 slice. The times are simulated.
256 devices in a mesh: ep: 64 (over z, y, core), tp: 4 (over x).
Axes of the slice: x: 4, y: 4, z: 8, core: 2. Of those that a mesh axis runs over, the one named last changes fastest.
Arguments:
- resid: bfloat16 [2048, 2048], P('ep'), may hold values from -6 to 6
- mix_gain: bfloat16 [2048], replicated, may hold values from 0.099609375 to 1.8984375
- proj_x: bfloat16 [2048, 512], P(None, 'tp'), may hold values from -0.125 to 0.125
- proj_z: bfloat16 [2048, 512], P(None, 'tp'), may hold values from -0.125 to 0.125
- proj_b: bfloat16 [2048, 512], P(None, 'tp'), may hold values from -0.125 to 0.125
- proj_c: bfloat16 [2048, 512], P(None, 'tp'), may hold values from -0.125 to 0.125
- proj_step: bfloat16 [2048, 8], replicated, may hold values from -0.125 to 0.125
- step_bias: float32 [8], P('tp'), may hold values from -5 to -1
- decay_rate: float32 [8], P('tp'), may hold values from 1 to 16
- conv_taps: bfloat16 [3, 4, 512], P(None, None, 'tp'), may hold values from -3 to 3
- conv_state: bfloat16 [2048, 3, 3, 512], P('ep', None, None, 'tp'), may hold values from -6 to 6
- scan_state: float32 [2048, 8, 64, 128], P('ep', 'tp'), may hold values from -2.5 to 2.5
- inner_gain: bfloat16 [512], P('tp'), may hold values from 0.099609375 to 1.8984375
- proj_out: bfloat16 [512, 2048], P('tp'), may hold values from -0.25 to 0.25
- post_gain: bfloat16 [2048], replicated, may hold values from 0.099609375 to 1.8984375
- ffn_gain: bfloat16 [2048], replicated, may hold values from 0.099609375 to 1.8984375
- group_router: bfloat16 [2048, 2], replicated, may hold values from -0.125 to 0.125
- expert_router: bfloat16 [2048, 64], replicated, may hold values from -0.125 to 0.125
- route_experts: int32 [2048, 4], P('ep'), may hold values from 0 to 63, as said below
- expert_gate: bfloat16 [64, 2048, 1024], P('ep', None, 'tp'), may hold values from -0.125 to 0.125
- expert_up: bfloat16 [64, 2048, 1024], P('ep', None, 'tp'), may hold values from -0.125 to 0.125
- expert_down: bfloat16 [64, 1024, 2048], P('ep', 'tp')
- dense_switch: bfloat16 [2048], replicated, may hold values from -0.125 to 0.125
- dense_gate: bfloat16 [2048, 2048], P('ep', 'tp'), may hold values from -0.125 to 0.125
- dense_up: bfloat16 [2048, 2048], P('ep', 'tp'), may hold values from -0.125 to 0.125
- dense_down: bfloat16 [2048, 2048], P('ep', 'tp')
- out_gain: bfloat16 [2048], P('tp'), may hold values from 0.099609375 to 1.8984375
Outputs:
- layer_out: bfloat16 [2048, 2048], P('ep', 'tp')
- new_state: float32 [2048, 8, 64, 128], P('ep', 'tp')
- new_conv: bfloat16 [2048, 3, 3, 512], P('ep', None, None, 'tp')
Inputs may be any that keep to these rules, and one draw needn't show every extreme that they name: `route_experts`: each row names 4 different experts, all from one group of 32 consecutive expert numbers. Within each aligned block of 32 rows (the rows of one index of ep) no expert is named more than 4 times, and one expert, the same in every block, is named exactly 4 times in every block.
All inputs are finite; a program needn't handle non-finite values.
Results may differ from a plain program's by a relative error of at most 0.019.
Values may be sent and summed in bfloat16 or wider, within the bound.
No kernel may reach another device: no remote copies, remote signals or barrier semaphores. Data moves between devices by JAX's collectives and lax.ppermute only.
A program may use at most 64 MiB of HBM per device.

v0:
```python
import jax
import jax.numpy as jnp
from jax import lax
from jax.sharding import Mesh
from jax.sharding import PartitionSpec as P

EP = ("ep_0", "ep_1", "ep_2")
norm_eps = 1e-06


def sent_to_all(array, axis):
    count = lax.axis_size(axis)
    return lax.all_to_all(
        jnp.broadcast_to(array[None], (count, *array.shape)), axis, 0, 0, tiled=True
    )


def taken_together(array, axis):
    return sent_to_all(array, axis).astype(jnp.float32).sum(axis=0)


def cut_along(array, dim, count):
    shape = array.shape
    pieces = array.reshape(*shape[:dim], count, shape[dim] // count, *shape[dim + 1 :])
    return jnp.moveaxis(pieces, dim, 0)


def sum_at_owner(array, axis, dim):
    count = lax.axis_size(axis)
    pieces = lax.all_to_all(cut_along(array, dim, count), axis, 0, 0, tiled=True)
    return jnp.sum(pieces.astype(jnp.float32), axis=0)


def laid_out(pieces, dim):
    shape = list(pieces.shape[1:])
    shape[dim] *= pieces.shape[0]
    return jnp.moveaxis(pieces, 0, dim).reshape(shape)


def exchange_in_order(pieces, axes, sequence):
    inside = pieces.shape[1:]
    result = pieces.reshape(*(lax.axis_size(a) for a in axes), *inside)
    for k in sequence:
        result = lax.all_to_all(result, axes[k], k, k, tiled=True)
    return result.reshape(-1, *inside)


def two_step_exchange(array, groups, sequence, split_dim, concat_dim):
    count = lax.axis_size(groups[0]) * lax.axis_size(groups[1])
    pieces = cut_along(array, split_dim, count)
    return laid_out(exchange_in_order(pieces, groups, sequence), concat_dim)


def gather_directly(array, axis, dim):
    return laid_out(sent_to_all(array, axis), dim)


def sent_together(arrays, axis, dim, along):
    widths = [a.shape[along] for a in arrays]
    both = jnp.concatenate(arrays, axis=along)
    result = lax.all_gather(both, axis, axis=dim, tiled=True)
    return tuple(jnp.split(result, [sum(widths[:k]) for k in range(1, len(widths))], axis=along))


def all_blocks(array, axes, sequence):
    pieces = array[None]
    for k in sequence:
        pieces = lax.all_gather(pieces, axes[k], axis=0, tiled=True)
    block = [lax.axis_size(axes[k]) for k in reversed(sequence)]
    pieces = pieces.reshape(*block, *array.shape)
    turned = sorted(range(len(sequence)), key=lambda place: sequence[len(sequence) - 1 - place])
    return pieces.transpose(*turned, *range(len(sequence), pieces.ndim)).reshape(-1, *array.shape)


def gathered_by_axis(array, axes, sequence, dim):
    return laid_out(all_blocks(array, axes, sequence), dim)


def taken_together_2(array, axis):
    return sent_to_all(array, axis).sum(axis=0)


def scaled_rows(values, gain):
    values = values.astype(jnp.float32)
    mean_square = jnp.mean(values * values, axis=-1, keepdims=True)
    return values * lax.rsqrt(mean_square + norm_eps) * gain.astype(jnp.float32)


def softmax_plain(logits):
    weights = jnp.exp(logits)
    return weights / jnp.sum(weights, axis=-1, keepdims=True)


def on_device(
    resid,
    mix_gain,
    proj_x,
    proj_z,
    proj_b,
    proj_c,
    proj_step,
    step_bias,
    decay_rate,
    conv_taps,
    conv_state,
    scan_state,
    inner_gain,
    proj_out,
    post_gain,
    ffn_gain,
    group_router,
    expert_router,
    route_experts,
    expert_gate,
    expert_up,
    expert_down,
    dense_switch,
    dense_gate,
    dense_up,
    dense_down,
    out_gain,
):
    tp_index = lax.axis_index("tp")
    seqs = resid.shape[0]
    width = resid.shape[1]
    quarter = width // lax.axis_size("tp")
    heads_here = scan_state.shape[1]
    head_dim = scan_state.shape[2]
    state_dim = scan_state.shape[3]
    channels = conv_state.shape[3]
    repeat = heads_here // (channels // state_dim)
    normed = scaled_rows(resid, mix_gain).astype(jnp.bfloat16)
    fresh = jnp.stack(
        [
            jnp.dot(normed, proj_x, preferred_element_type=jnp.float32),
            jnp.dot(normed, proj_b, preferred_element_type=jnp.float32),
            jnp.dot(normed, proj_c, preferred_element_type=jnp.float32),
        ],
        axis=1,
    ).astype(jnp.bfloat16)
    gate_z = jnp.dot(normed, proj_z, preferred_element_type=jnp.float32)
    step_all = jnp.dot(normed, proj_step, preferred_element_type=jnp.float32)
    step_raw = lax.dynamic_slice_in_dim(step_all, tp_index * heads_here, heads_here, 1)
    history = jnp.concatenate([conv_state, fresh[:, :, None, :]], axis=2)
    activated = jax.nn.silu(
        jnp.sum(history.astype(jnp.float32) * conv_taps.astype(jnp.float32)[None], axis=2)
    )
    xs_heads = activated[:, 0].reshape(seqs, heads_here, head_dim)
    b_heads = jnp.repeat(activated[:, 1].reshape(seqs, -1, state_dim), repeat, axis=1)
    c_heads = jnp.repeat(activated[:, 2].reshape(seqs, -1, state_dim), repeat, axis=1)
    step = jax.nn.softplus(step_raw + step_bias)
    keep = jnp.exp(-decay_rate * step)
    driven = step[:, :, None] * xs_heads
    new_state = keep[:, :, None, None] * scan_state + driven[:, :, :, None] * b_heads[:, :, None, :]
    read = jnp.sum(new_state * c_heads[:, :, None, :], axis=3).reshape(seqs, channels)
    gated = (read * jax.nn.silu(gate_z) * inner_gain.astype(jnp.float32)).astype(jnp.bfloat16)
    mixed = taken_together(
        jnp.dot(gated, proj_out, preferred_element_type=jnp.float32).astype(jnp.bfloat16), "tp"
    ).astype(jnp.float32)
    stream = (resid.astype(jnp.float32) + scaled_rows(mixed, post_gain)).astype(jnp.bfloat16)
    feed = scaled_rows(stream, ffn_gain).astype(jnp.bfloat16)
    feed_quarter = lax.dynamic_slice_in_dim(feed, tp_index * quarter, quarter, 1)
    expert_count = expert_router.shape[1]
    group_size = expert_count // group_router.shape[1]
    pick_count = route_experts.shape[1]
    group_prob = softmax_plain(jnp.dot(feed, group_router, preferred_element_type=jnp.float32))
    expert_logits = jnp.dot(feed, expert_router, preferred_element_type=jnp.float32)
    matches = route_experts[:, :, None] == jnp.arange(expert_count, dtype=jnp.int32)[None, None, :]
    pick_logits = jnp.sum(jnp.where(matches, expert_logits[:, None, :], 0.0), axis=2)
    chosen_group = route_experts[:, 0] // group_size
    group_ids = jnp.arange(group_router.shape[1], dtype=jnp.int32)
    group_weight = jnp.sum(
        jnp.where(chosen_group[:, None] == group_ids[None, :], group_prob, 0.0), axis=1
    )
    pick_weight = softmax_plain(pick_logits) * group_weight[:, None]
    capacity = 2 * seqs * pick_count // expert_count
    flat_picks = route_experts.reshape(-1)
    one_hot = (flat_picks[:, None] == jnp.arange(expert_count, dtype=jnp.int32)[None, :]).astype(
        jnp.int32
    )
    slot = jnp.sum((jnp.cumsum(one_hot, axis=0) - one_hot) * one_hot, axis=1)
    target = flat_picks * capacity + slot
    repeated = jnp.repeat(feed_quarter, pick_count, axis=0)
    outgoing = jnp.zeros((expert_count * capacity, quarter), jnp.bfloat16).at[target].set(repeated)
    outgoing = outgoing.reshape(expert_count, capacity, quarter)
    arrived = gather_directly(
        lax.all_to_all(outgoing, EP, split_axis=0, concat_axis=0, tiled=True), "tp", 2
    )
    sources = arrived.shape[0]
    items = arrived.shape[1]
    rows = arrived.reshape(sources * items, width)
    gate_value = jnp.dot(rows, expert_gate[0], preferred_element_type=jnp.float32)
    up_value = jnp.dot(rows, expert_up[0], preferred_element_type=jnp.float32)
    hidden = (jax.nn.silu(gate_value) * up_value).astype(jnp.bfloat16)
    result = jnp.dot(hidden, expert_down[0], preferred_element_type=jnp.float32).reshape(
        sources, items, width
    )
    summed = sum_at_owner(result.astype(jnp.bfloat16), "tp", 2)
    returned = two_step_exchange(
        summed.astype(jnp.bfloat16), (("ep_0", "ep_1"), "ep_2"), (1, 0), 0, 0
    )
    fetched = returned.reshape(expert_count * capacity, quarter)[target].reshape(
        seqs, pick_count, quarter
    )
    routed = jnp.sum(fetched.astype(jnp.float32) * pick_weight[:, :, None], axis=1)
    pieces = sent_together((dense_gate, dense_up), EP, 0, 1)
    gate_piece = jnp.einsum(
        "sd,cd->sc", feed_quarter, pieces[0], preferred_element_type=jnp.float32
    )
    up_piece = jnp.einsum("sd,cd->sc", feed_quarter, pieces[1], preferred_element_type=jnp.float32)
    gate_sum = gate_piece
    up_sum = up_piece
    gate_sum, up_sum = (
        taken_together(gate_sum.astype(jnp.bfloat16), "tp").astype(jnp.float32),
        taken_together(up_sum.astype(jnp.bfloat16), "tp").astype(jnp.float32),
    )
    dense_hidden = (jax.nn.silu(gate_sum) * up_sum).astype(jnp.bfloat16)
    dense_out = jnp.dot(
        dense_hidden,
        gathered_by_axis(dense_down, EP, (1, 0, 2), 0),
        preferred_element_type=jnp.float32,
    )
    switch = jax.nn.sigmoid(jnp.dot(feed, dense_switch, preferred_element_type=jnp.float32))
    combined = routed + switch[:, None] * dense_out
    total_square = taken_together_2(jnp.sum(combined * combined, axis=1), "tp")
    scale = lax.rsqrt(total_square / width + norm_eps)
    stream_part = lax.dynamic_slice_in_dim(stream, tp_index * quarter, quarter, 1).astype(
        jnp.float32
    )
    layer_out = (stream_part + combined * scale[:, None] * out_gain.astype(jnp.float32)).astype(
        jnp.bfloat16
    )
    new_conv = history[:, :, 1:, :]
    return (layer_out, new_state, new_conv)


def solution(mesh):
    torus = Mesh(mesh.devices.reshape(8, 4, 2, mesh.shape["tp"]), ("ep_0", "ep_1", "ep_2", "tp"))
    in_specs = (
        P(EP, None),
        P(),
        P(None, "tp"),
        P(None, "tp"),
        P(None, "tp"),
        P(None, "tp"),
        P(),
        P("tp"),
        P("tp"),
        P(None, None, "tp"),
        P(EP, None, None, "tp"),
        P(EP, "tp", None, None),
        P("tp"),
        P("tp", None),
        P(),
        P(),
        P(),
        P(),
        P(EP, None),
        P(EP, None, "tp"),
        P(EP, None, "tp"),
        P(EP, "tp", None),
        P(),
        P(EP, "tp"),
        P(EP, "tp"),
        P(EP, "tp"),
        P("tp"),
    )
    out_specs = (P(EP, "tp"), P(EP, "tp", None, None), P(EP, None, None, "tp"))
    return jax.shard_map(
        on_device, mesh=torus, in_specs=in_specs, out_specs=out_specs, check_vma=False
    )
```

profile of v0, /device:TPU:32, one launch (start us, length us, event | category | flops | bytes accessed | tf_op | source)
XLA Modules:
  0.0 196.0 jit_solution(9819140083257767766)
XLA Ops:
  7.3 14.3 %all-gather = bf16[128,512]{1,0:T(8,128)(2,1)} all-gather(bf16[32,512]{1,0:T(8,128)(2,1)} %param.52), channel_id=2, replica_groups=mesh['ep_0'=8,'ep_1'=4,'ep_2'=2,'tp'=4] {'ep_1'}, dimensions={0}, use_global_device_ids=true | all-gather | bytes 163840 | tf_op jit(solution)/shard_map/all_gather | solution.py:68
  31.2 2.1 %multiply_reduce_fusion = (f32[32,2,64]{2,1,0:T(2,128)S(1)}, f32[32,2,64,128]{3,2,1,0:T(8,128)}) fusion(f32[32,128]{1,0:T(8,128)S(1)} %get-tuple-element.12, f32[32,128]{1,0:T(8,128)S(1)} %get-tuple-element.13, f32[32,2,64]{2,1,0:T(2,128)S(1)} %broadcast_multiply_fusion, f32[32,2,64,128]{3,2,1,0:T(8,128)S(1)} %copy-done.2, f32[32,2]{1,0:T(8,128)S(1)} %copy.73), kind=kLoop, calls=%fused_computation.8 | loop fusion | flops 2617344 | bytes 4260096 | tf_op jit(solution)/shard_map/reduce_sum | solution.py:155
  33.5 1.7 convolution_convert_fusion.3
  36.0 4.3 %all-to-all-start = ((bf16[4,32,2048]{2,1,0:T(8,128)(2,1)}), bf16[4,32,2048]{2,1,0:T(8,128)(2,1)S(1)}, u32[]{:S(2)}, u32[]{:S(2)}) async-start(bf16[4,32,2048]{2,1,0:T(8,128)(2,1)} %broadcast_in_dim.25), calls=%async_computation | async-start | bytes 1048576 | tf_op jit(solution)/shard_map/all_to_all | solution.py:13
  41.2 7.2 %all-to-all-done = bf16[4,32,2048]{2,1,0:T(8,128)(2,1)S(1)} async-done(((bf16[4,32,2048]{2,1,0:T(8,128)(2,1)}), bf16[4,32,2048]{2,1,0:T(8,128)(2,1)S(1)}, u32[]{:S(2)}, u32[]{:S(2)}) %all-to-all-start) | async-done | bytes 524320 | tf_op jit(solution)/shard_map/all_to_all | solution.py:13
  50.3 22.3 %all_to_all.46 = bf16[64,4,512]{2,1,0:T(4,128)(2,1)S(1)} all-to-all(bf16[64,4,512]{2,1,0:T(4,128)(2,1)S(1)} %reshape.201), channel_id=1, replica_groups=mesh['ep_0'=8,'ep_1'=4,'ep_2'=2,'tp'=4] {'ep_0','ep_1','ep_2'}, dimensions={0} | all-to-all | bytes 524288 | tf_op jit(solution)/shard_map/all_to_all | solution.py:187
  72.9 18.5 %all_to_all.47 = bf16[4,64,4,512]{3,2,1,0:T(4,128)(2,1)S(1)} all-to-all(bf16[4,64,4,512]{3,2,1,0:T(4,128)(2,1)S(1)} %broadcast_in_dim.28), channel_id=1, replica_groups=mesh['ep_0'=8,'ep_1'=4,'ep_2'=2,'tp'=4] {'tp'}, dimensions={0} | all-to-all | bytes 2097152 | tf_op jit(solution)/shard_map/all_to_all | solution.py:13
  96.0 3.6 %all-to-all-start.3 = ((bf16[4,64,4,512]{3,1,2,0:T(8,128)(2,1)}), bf16[4,64,4,512]{3,1,2,0:T(8,128)(2,1)S(1)}, u32[]{:S(2)}, u32[]{:S(2)}) async-start(bf16[4,64,4,512]{3,1,2,0:T(8,128)(2,1)} %bitcast.77), calls=%async_computation.3 | async-start | bytes 2097152 | tf_op jit(solution)/shard_map/all_to_all | solution.py:30
  100.8 13.7 %all-to-all-done.3 = bf16[4,64,4,512]{3,1,2,0:T(8,128)(2,1)S(1)} async-done(((bf16[4,64,4,512]{3,1,2,0:T(8,128)(2,1)}), bf16[4,64,4,512]{3,1,2,0:T(8,128)(2,1)S(1)}, u32[]{:S(2)}, u32[]{:S(2)}) %all-to-all-start.3) | async-done | bytes 1048608 | tf_op jit(solution)/shard_map/all_to_all | solution.py:30
  115.1 3.9 %all_to_all.48 = bf16[32,2,1,4,512]{4,3,0,2,1:T(4,128)(2,1)S(1)} all-to-all(bf16[32,2,1,4,512]{4,3,0,2,1:T(4,128)(2,1)S(1)} %copy.81), channel_id=1, replica_groups=mesh['ep_0'=8,'ep_1'=4,'ep_2'=2,'tp'=4] {'ep_2'}, dimensions={1} | all-to-all | bytes 524288 | tf_op jit(solution)/shard_map/all_to_all | solution.py:44
  119.8 4.6 %all-to-all-start.5 = ((bf16[32,2,1,4,512]{4,3,1,2,0:T(4,128)(2,1)}), bf16[32,2,1,4,512]{4,3,1,2,0:T(4,128)(2,1)S(1)}, u32[]{:S(2)}, u32[]{:S(2)}) async-start(bf16[32,2,1,4,512]{4,3,1,2,0:T(4,128)(2,1)} %copy.82), calls=%async_computation.5 | async-start | bytes 524288 | tf_op jit(solution)/shard_map/all_to_all | solution.py:44
  124.6 19.8 %all-gather.5.cloned.1.call-done = bf16[2048,1024]{1,0:T(8,128)(2,1)} async-done(((bf16[32,1024]{1,0:T(8,128)(2,1)}), bf16[2048,1024]{1,0:T(8,128)(2,1)}) %all-gather.5.cloned.1.call-update) | async-done | bytes 4194320 | tf_op jit(solution)/shard_map/all_gather | solution.py:61
  144.4 2.3 %convolution_convert_fusion.1 = bf16[32,2048]{1,0:T(8,128)(2,1)S(1)} fusion(bf16[32,512]{1,0:T(8,128)(2,1)S(1)} %constant_dynamic-slice_fusion, bf16[2048,1024]{1,0:T(8,128)(2,1)} %all-gather.5.cloned.1.call-done), kind=kOutput, calls=%fused_computation.3 | convolution fusion | flops 67174400 | bytes 2260992 | tf_op jit(solution)/shard_map/sd,cd->sc/dot_general | solution.py:210
  147.6 4.2 %all-to-all-start.7 = ((bf16[4,32,2048]{2,1,0:T(8,128)(2,1)}), bf16[4,32,2048]{2,1,0:T(8,128)(2,1)S(1)}, u32[]{:S(2)}, u32[]{:S(2)}) async-start(bf16[4,32,2048]{2,1,0:T(8,128)(2,1)} %broadcast_in_dim.37), calls=%async_computation.7 | async-start | bytes 1048576 | tf_op jit(solution)/shard_map/all_to_all | solution.py:13
  151.9 2.3 %convolution_convert_fusion.2 = bf16[32,2048]{1,0:T(8,128)(2,1)S(1)} fusion(bf16[32,512]{1,0:T(8,128)(2,1)S(1)} %constant_dynamic-slice_fusion, bf16[2048,1024]{1,0:T(8,128)(2,1)} %all-gather.5.cloned.1.call-done), kind=kOutput, calls=%fused_computation.4 | convolution fusion | flops 67174400 | bytes 2260992 | tf_op jit(solution)/shard_map/sd,cd->sc/dot_general | solution.py:207
  154.2 7.5 %all-to-all-done.7 = bf16[4,32,2048]{2,1,0:T(8,128)(2,1)S(1)} async-done(((bf16[4,32,2048]{2,1,0:T(8,128)(2,1)}), bf16[4,32,2048]{2,1,0:T(8,128)(2,1)S(1)}, u32[]{:S(2)}, u32[]{:S(2)}) %all-to-all-start.7) | async-done | bytes 524320 | tf_op jit(solution)/shard_map/all_to_all | solution.py:13
  162.6 4.1 %all-to-all-start.6 = ((bf16[4,32,2048]{2,1,0:T(8,128)(2,1)}), bf16[4,32,2048]{2,1,0:T(8,128)(2,1)}, u32[]{:S(2)}, u32[]{:S(2)}) async-start(bf16[4,32,2048]{2,1,0:T(8,128)(2,1)} %broadcast_in_dim.35), calls=%async_computation.6 | async-start | bytes 1048576 | tf_op jit(solution)/shard_map/all_to_all | solution.py:13
  168.8 1.8 copy.84
  170.7 5.1 %all-to-all-done.6 = bf16[4,32,2048]{2,1,0:T(8,128)(2,1)} async-done(((bf16[4,32,2048]{2,1,0:T(8,128)(2,1)}), bf16[4,32,2048]{2,1,0:T(8,128)(2,1)}, u32[]{:S(2)}, u32[]{:S(2)}) %all-to-all-start.6) | async-done | bytes 524320 | tf_op jit(solution)/shard_map/all_to_all | solution.py:13
  176.9 2.0 %multiply_reduce_fusion.4 = (f32[32]{0:T(128)S(1)}, f32[32,512]{1,0:T(8,128)}) fusion(f32[32,512]{1,0:T(8,128)} %multiply_reduce_fusion.1, bf16[2048,512]{1,0:T(8,128)(2,1)S(1)} %bitcast.78, f32[32,2048]{1,0:T(8,128)S(1)} %convert_reduce_fusion, f32[32,2048]{1,0:T(8,128)S(1)} %convert_reduce_fusion.1, f32[32]{0:T(128)S(1)} %fusion.10), kind=kOutput, calls=%fused_computation.57 | convolution fusion | flops 67567584 | bytes 2752768 | tf_op jit(solution)/shard_map/dot_general | solution.py:218
  179.5 3.2 %all-to-all-start.8 = ((f32[4,1,32]{2,1,0:T(1,128)}), f32[4,1,32]{2,1,0:T(1,128)S(1)}, u32[]{:S(2)}, u32[]{:S(2)}) async-start(f32[4,1,32]{2,1,0:T(1,128)} %broadcast_in_dim.39), calls=%async_computation.8 | async-start | bytes 4096 | tf_op jit(solution)/shard_map/all_to_all | solution.py:13
  182.7 1.5 slice.31
  184.3 3.6 %all-to-all-done.8 = f32[4,1,32]{2,1,0:T(1,128)S(1)} async-done(((f32[4,1,32]{2,1,0:T(1,128)}), f32[4,1,32]{2,1,0:T(1,128)S(1)}, u32[]{:S(2)}, u32[]{:S(2)}) %all-to-all-start.8) | async-done | bytes 544 | tf_op jit(solution)/shard_map/all_to_all | solution.py:13
  187.9 1.5 add_convert_fusion
  (125 shorter events, 26.4 us)
Async XLA Ops:
  7.2 87.3 %copy-start = (bf16[1,256,2048]{2,1,0:T(8,128)(2,1)S(1)}, bf16[1,256,2048]{2,1,0:T(8,128)(2,1)}, u32[]{:S(2)}) copy-start(bf16[1,256,2048]{2,1,0:T(8,128)(2,1)} %param.48) | copy-start | bytes 3145732
  7.2 23.4 %copy-start.1 = (bf16[32,2048]{1,0:T(8,128)(2,1)S(1)}, bf16[32,2048]{1,0:T(8,128)(2,1)}, u32[]{:S(2)}) copy-start(bf16[32,2048]{1,0:T(8,128)(2,1)} %param.27) | copy-start | bytes 393220
  7.2 22.5 %copy-start.7 = (bf16[32,3,3,128]{3,0,2,1:T(8,128)(2,1)S(1)}, bf16[32,3,3,128]{3,0,2,1:T(8,128)(2,1)}, u32[]{:S(2)}) copy-start(bf16[32,3,3,128]{3,0,2,1:T(8,128)(2,1)} %param.37) | copy-start | bytes 221188
  7.2 23.3 %copy-start.17 = (f32[2]{0:T(128)S(1)}, f32[2]{0:T(128)}, u32[]{:S(2)}) copy-start(f32[2]{0:T(128)} %param.35) | copy-start | bytes 28
  7.2 23.4 %copy-start.15 = (bf16[2048,8]{0,1:T(8,128)(2,1)S(1)}, bf16[2048,8]{0,1:T(8,128)(2,1)}, u32[]{:S(2)}) copy-start(bf16[2048,8]{0,1:T(8,128)(2,1)} %param.33) | copy-start | bytes 98308
  7.2 23.6 %copy-start.13 = (f32[2]{0:T(128)S(1)}, f32[2]{0:T(128)}, u32[]{:S(2)}) copy-start(f32[2]{0:T(128)} %param.34) | copy-start | bytes 28
  7.2 24.0 %copy-start.2 = (f32[32,2,64,128]{3,2,1,0:T(8,128)S(1)}, f32[32,2,64,128]{3,2,1,0:T(8,128)}, u32[]{:S(2)}) copy-start(f32[32,2,64,128]{3,2,1,0:T(8,128)} %param.38) | copy-start | bytes 6291460
  7.2 92.5 %all-gather.7.cloned.1.call-start = ((), (), s32[]{:S(2)}) async-start(), calls=%async_computation.10 | async-start | bytes 1179648 | tf_op jit(solution)/shard_map/all_gather | solution.py:68
  21.7 122.8 %all-gather.5.cloned.1.call-start = ((), (), s32[]{:S(2)}) async-start(), calls=%async_computation.9 | async-start | bytes 4259840 | tf_op jit(solution)/shard_map/all_gather | solution.py:61
  33.3 7.0 %copy-start.8 = (s32[32,4]{0,1:T(4,128)S(1)}, s32[32,4]{0,1:T(4,128)}, u32[]{:S(2)}) copy-start(s32[32,4]{0,1:T(4,128)} %param.45) | copy-start | bytes 1540
  33.3 7.3 %copy-start.9 = (bf16[2048]{0:T(1024)(128)(2,1)S(1)}, bf16[2048]{0:T(1024)(128)(2,1)}, u32[]{:S(2)}) copy-start(bf16[2048]{0:T(1024)(128)(2,1)} %param.41) | copy-start | bytes 12292
  33.4 7.3 %copy-start.10 = (bf16[2048]{0:T(1024)(128)(2,1)S(1)}, bf16[2048]{0:T(1024)(128)(2,1)}, u32[]{:S(2)}) copy-start(bf16[2048]{0:T(1024)(128)(2,1)} %param.42) | copy-start | bytes 12292
  36.0 12.4 %all-to-all-start = ((bf16[4,32,2048]{2,1,0:T(8,128)(2,1)}), bf16[4,32,2048]{2,1,0:T(8,128)(2,1)S(1)}, u32[]{:S(2)}, u32[]{:S(2)}) async-start(bf16[4,32,2048]{2,1,0:T(8,128)(2,1)} %broadcast_in_dim.25), calls=%async_computation | async-start | bytes 1048576 | tf_op jit(solution)/shard_map/all_to_all | solution.py:13
  96.0 4.4 %copy-start.11 = (bf16[2048]{0:T(1024)(128)(2,1)S(1)}, bf16[2048]{0:T(1024)(128)(2,1)}, u32[]{:S(2)}) copy-start(bf16[2048]{0:T(1024)(128)(2,1)} %param.49) | copy-start | bytes 12292
  96.0 4.5 %copy-start.16 = (bf16[2048,2]{0,1:T(2,128)(2,1)S(1)}, bf16[2048,2]{0,1:T(2,128)(2,1)}, u32[]{:S(2)}) copy-start(bf16[2048,2]{0,1:T(2,128)(2,1)} %param.43) | copy-start | bytes 24580
  96.0 4.6 %copy-start.6 = (bf16[2048,64]{0,1:T(8,128)(2,1)S(1)}, bf16[2048,64]{0,1:T(8,128)(2,1)}, u32[]{:S(2)}) copy-start(bf16[2048,64]{0,1:T(8,128)(2,1)} %param.44) | copy-start | bytes 786436
  96.0 18.6 %all-to-all-start.3 = ((bf16[4,64,4,512]{3,1,2,0:T(8,128)(2,1)}), bf16[4,64,4,512]{3,1,2,0:T(8,128)(2,1)S(1)}, u32[]{:S(2)}, u32[]{:S(2)}) async-start(bf16[4,64,4,512]{3,1,2,0:T(8,128)(2,1)} %bitcast.77), calls=%async_computation.3 | async-start | bytes 2097152 | tf_op jit(solution)/shard_map/all_to_all | solution.py:30
  99.7 69.1 %all-gather.9.cloned.1.call-start = ((), (), s32[]{:S(2)}) async-start(), calls=%async_computation.11 | async-start | bytes 3145728 | tf_op jit(solution)/shard_map/all_gather | solution.py:68
  119.8 26.9 %all-to-all-start.5 = ((bf16[32,2,1,4,512]{4,3,1,2,0:T(4,128)(2,1)}), bf16[32,2,1,4,512]{4,3,1,2,0:T(4,128)(2,1)S(1)}, u32[]{:S(2)}, u32[]{:S(2)}) async-start(bf16[32,2,1,4,512]{4,3,1,2,0:T(4,128)(2,1)} %copy.82), calls=%async_computation.5 | async-start | bytes 524288 | tf_op jit(solution)/shard_map/all_to_all | solution.py:44
  147.6 14.1 %all-to-all-start.7 = ((bf16[4,32,2048]{2,1,0:T(8,128)(2,1)}), bf16[4,32,2048]{2,1,0:T(8,128)(2,1)S(1)}, u32[]{:S(2)}, u32[]{:S(2)}) async-start(bf16[4,32,2048]{2,1,0:T(8,128)(2,1)} %broadcast_in_dim.37), calls=%async_computation.7 | async-start | bytes 1048576 | tf_op jit(solution)/shard_map/all_to_all | solution.py:13
  161.6 5.1 %copy-start.3 = (bf16[4,32,2048]{2,1,0:T(8,128)(2,1)}, bf16[4,32,2048]{2,1,0:T(8,128)(2,1)S(1)}, u32[]{:S(2)}) copy-start(bf16[4,32,2048]{2,1,0:T(8,128)(2,1)S(1)} %all-to-all-done.7) | copy-start | bytes 1572868
  162.6 13.2 %all-to-all-start.6 = ((bf16[4,32,2048]{2,1,0:T(8,128)(2,1)}), bf16[4,32,2048]{2,1,0:T(8,128)(2,1)}, u32[]{:S(2)}, u32[]{:S(2)}) async-start(bf16[4,32,2048]{2,1,0:T(8,128)(2,1)} %broadcast_in_dim.35), calls=%async_computation.6 | async-start | bytes 1048576 | tf_op jit(solution)/shard_map/all_to_all | solution.py:13
  170.6 12.2 %copy-start.12 = (bf16[512]{0:T(512)(128)(2,1)S(1)}, bf16[512]{0:T(512)(128)(2,1)}, u32[]{:S(2)}) copy-start(bf16[512]{0:T(512)(128)(2,1)} %param.53) | copy-start | bytes 3076
  179.5 8.4 %all-to-all-start.8 = ((f32[4,1,32]{2,1,0:T(1,128)}), f32[4,1,32]{2,1,0:T(1,128)S(1)}, u32[]{:S(2)}, u32[]{:S(2)}) async-start(f32[4,1,32]{2,1,0:T(1,128)} %broadcast_in_dim.39), calls=%async_computation.8 | async-start | bytes 4096 | tf_op jit(solution)/shard_map/all_to_all | solution.py:13
  (4 other events, 6.9 us)
Sparse Core Ops, SparseCore 0:
  21.8 38.9 all-gather.6
  64.1 80.2 all-gather.4
  146.2 13.5 all-gather.8
where the time goes:
time: 197 us; the launch traced here: 196 us
  blocking collectives  59.1 us (30%)
  waiting for transfers between devices  57.6 us (29%)
  starting transfers between devices  24.2 us (12%)
  matrix products  14.5 us (7%)
  local copies, waits for them, and re-layouts  14.4 us (7%)
  between operations  14.3 us (7%)
  other arithmetic  12 us (6%)
    all_to_all x4, waiting for transfers between devices, sent_to_all(): lax.all_to_all(jnp.broadcast_to(array[None], (count, *array.shape)), axis...  23.4 us
    all_to_all x1, blocking collectives, on_device(): lax.all_to_all(outgoing, EP, split_axis=0, concat_axis=0, tiled=True)  22.3 us
    all_gather x1, waiting for transfers between devices, sent_together(): result = lax.all_gather(both, axis, axis=dim, tiled=True)  19.8 us
    all_to_all x1, blocking collectives, sent_to_all(): lax.all_to_all(jnp.broadcast_to(array[None], (count, *array.shape)), axis...  18.5 us
    all_to_all x4, starting transfers between devices, sent_to_all(): lax.all_to_all(jnp.broadcast_to(array[None], (count, *array.shape)), axis...  15.8 us
    all_gather x1, blocking collectives, all_blocks(): pieces = lax.all_gather(pieces, axes[k], axis=0, tiled=True)  14.3 us
    all_to_all x1, waiting for transfers between devices, sum_at_owner(): lax.all_to_all(cut_along(array, dim, count), axis, 0, 0, tiled=True)  13.7 us
    all_to_all x1, starting transfers between devices, exchange_in_order(): result = lax.all_to_all(result, axes[k], k, k, tiled=True)  4.58 us
  transfers between devices with their start and end apart: 9, of which 6 were waited for; matrix products, arithmetic and copies ran while one was open for 18% of the time, Pallas kernels for 0%

commit v1 on v0

--- a/solution.py
+++ b/solution.py
@@ -65,7 +65,9 @@
 def all_blocks(array, axes, sequence):
     pieces = array[None]
     for k in sequence:
-        pieces = lax.all_gather(pieces, axes[k], axis=0, tiled=True)
+        pieces = jnp.concatenate(
+            lax.all_to_all(jnp.stack([pieces] * lax.axis_size(axes[k])), axes[k], 0, 0), axis=0
+        )
     block = [lax.axis_size(axes[k]) for k in reversed(sequence)]
     pieces = pieces.reshape(*block, *array.shape)
     turned = sorted(range(len(sequence)), key=lambda place: sequence[len(sequence) - 1 - place])

time: 197 us -> 218 us (1.11)
  starting transfers between devices: 24.2 us -> 40.2 us
  blocking collectives: 59.1 us -> 44.2 us
  local copies, waits for them, and re-layouts: 14.4 us -> 20.5 us
  other arithmetic: 12 us -> 17.1 us
  matrix products: 14.5 us -> 18.8 us
  waiting for transfers between devices: 57.6 us -> 61.1 us
    all_to_all x0 -> x3, waiting for transfers between devices: none -> 28 us  [all_blocks(): lax.all_to_all(jnp.stack([pieces] * lax.axis_size(axes[k])), axes[k], 0, 0)]
    all_gather x1, waiting for transfers between devices: 19.8 us -> 0.02 us  [sent_together(): result = lax.all_gather(both, axis, axis=dim, tiled=True)]
    all_gather x1 -> x0, blocking collectives: 14.3 us -> none  [all_blocks(): pieces = lax.all_gather(pieces, axes[k], axis=0, tiled=True)]
    all_to_all x0 -> x3, starting transfers between devices: none -> 12.5 us  [all_blocks(): lax.all_to_all(jnp.stack([pieces] * lax.axis_size(axes[k])), axes[k], 0, 0)]
    all_to_all x1, waiting for transfers between devices: 0.02 us -> 7.68 us  [exchange_in_order(): result = lax.all_to_all(result, axes[k], k, k, tiled=True)]
    all_to_all x1, waiting for transfers between devices: 13.7 us -> 7.22 us  [sum_at_owner(): lax.all_to_all(cut_along(array, dim, count), axis, 0, 0, tiled=True)]
    all_to_all x4, waiting for transfers between devices: 23.4 us -> 18.1 us  [sent_to_all(): lax.all_to_all(jnp.broadcast_to(array[None], (count, *array.shape)), axis...]
    all_to_all x1, starting transfers between devices: 4.58 us -> 7.84 us  [exchange_in_order(): result = lax.all_to_all(result, axes[k], k, k, tiled=True)]
  transfers between devices with their start and end apart: 9 -> 10, of which waited for: 6 -> 9; matrix products, arithmetic and copies ran while one was open for 18% -> 20% of each run, Pallas kernels for 0% -> 0%
where the time goes in v1:
time: 218 us; the launch traced here: 216 us
  waiting for transfers between devices  61.1 us (28%)
  blocking collectives  44.2 us (20%)
  starting transfers between devices  40.2 us (18%)
  local copies, waits for them, and re-layouts  20.5 us (9%)
  matrix products  18.8 us (9%)
  other arithmetic  17.1 us (8%)
  between operations  14.6 us (7%)
    all_to_all x3, waiting for transfers between devices, all_blocks(): lax.all_to_all(jnp.stack([pieces] * lax.axis_size(axes[k])), axes[k], 0, 0)  28 us
    all_to_all x1, blocking collectives, on_device(): lax.all_to_all(outgoing, EP, split_axis=0, concat_axis=0, tiled=True)  21.7 us
    all_to_all x1, blocking collectives, sent_to_all(): lax.all_to_all(jnp.broadcast_to(array[None], (count, *array.shape)), axis...  18.5 us
    all_to_all x4, waiting for transfers between devices, sent_to_all(): lax.all_to_all(jnp.broadcast_to(array[None], (count, *array.shape)), axis...  18.1 us
    all_to_all x4, starting transfers between devices, sent_to_all(): lax.all_to_all(jnp.broadcast_to(array[None], (count, *array.shape)), axis...  16.3 us
    all_to_all x3, starting transfers between devices, all_blocks(): lax.all_to_all(jnp.stack([pieces] * lax.axis_size(axes[k])), axes[k], 0, 0)  12.5 us
    all_to_all x1, starting transfers between devices, exchange_in_order(): result = lax.all_to_all(result, axes[k], k, k, tiled=True)  7.84 us
    all_to_all x1, waiting for transfers between devices, exchange_in_order(): result = lax.all_to_all(result, axes[k], k, k, tiled=True)  7.68 us
  transfers between devices with their start and end apart: 10, of which 9 were waited for; matrix products, arithmetic and copies ran while one was open for 20% of the time, Pallas kernels for 0%

profile of v1, /device:TPU:32, one launch (start us, length us, event | category | flops | bytes accessed | tf_op | source)
XLA Modules:
  0.0 216.5 jit_solution(9226051589314237836)
XLA Ops:
  16.3 2.1 multiply_reduce_fusion
  21.1 4.3 %all-to-all-start = ((bf16[4,32,2048]{2,1,0:T(8,128)(2,1)}), bf16[4,32,2048]{2,1,0:T(8,128)(2,1)S(1)}, u32[]{:S(2)}, u32[]{:S(2)}) async-start(bf16[4,32,2048]{2,1,0:T(8,128)(2,1)} %broadcast_in_dim.23), calls=%async_computation | async-start | bytes 1048576 | tf_op jit(solution)/shard_map/all_to_all | solution.py:13
  26.3 8.6 %all-to-all-done = bf16[4,32,2048]{2,1,0:T(8,128)(2,1)S(1)} async-done(((bf16[4,32,2048]{2,1,0:T(8,128)(2,1)}), bf16[4,32,2048]{2,1,0:T(8,128)(2,1)S(1)}, u32[]{:S(2)}, u32[]{:S(2)}) %all-to-all-start) | async-done | bytes 524320 | tf_op jit(solution)/shard_map/all_to_all | solution.py:13
  35.5 4.5 %all-to-all-start.8 = ((bf16[4,1,32,512]{3,2,1,0:T(8,128)(2,1)}), bf16[4,1,32,512]{3,2,1,0:T(8,128)(2,1)S(1)}, u32[]{:S(2)}, u32[]{:S(2)}) async-start(bf16[4,1,32,512]{3,2,1,0:T(8,128)(2,1)} %stack.25), calls=%async_computation.8 | async-start | bytes 262144 | tf_op jit(solution)/shard_map/all_to_all | solution.py:69
  42.4 3.5 %all-to-all-done.8 = bf16[4,1,32,512]{3,2,1,0:T(8,128)(2,1)S(1)} async-done(((bf16[4,1,32,512]{3,2,1,0:T(8,128)(2,1)}), bf16[4,1,32,512]{3,2,1,0:T(8,128)(2,1)S(1)}, u32[]{:S(2)}, u32[]{:S(2)}) %all-to-all-start.8) | async-done | bytes 131104 | tf_op jit(solution)/shard_map/all_to_all | solution.py:69
  45.9 21.7 %all_to_all.61 = bf16[64,4,512]{2,1,0:T(4,128)(2,1)S(1)} all-to-all(bf16[64,4,512]{2,1,0:T(4,128)(2,1)S(1)} %reshape.202), channel_id=1, replica_groups=mesh['ep_0'=8,'ep_1'=4,'ep_2'=2,'tp'=4] {'ep_0','ep_1','ep_2'}, dimensions={0} | all-to-all | bytes 524288 | tf_op jit(solution)/shard_map/all_to_all | solution.py:189
  67.9 18.5 %all_to_all.62 = bf16[4,64,4,512]{3,2,1,0:T(4,128)(2,1)S(1)} all-to-all(bf16[4,64,4,512]{3,2,1,0:T(4,128)(2,1)S(1)} %broadcast_in_dim.26), channel_id=1, replica_groups=mesh['ep_0'=8,'ep_1'=4,'ep_2'=2,'tp'=4] {'tp'}, dimensions={0} | all-to-all | bytes 2097152 | tf_op jit(solution)/shard_map/all_to_all | solution.py:13
  87.5 4.3 %all-to-all-start.9 = ((bf16[8,4,32,512]{3,2,1,0:T(8,128)(2,1)}), bf16[8,4,32,512]{3,2,1,0:T(8,128)(2,1)S(1)}, u32[]{:S(2)}, u32[]{:S(2)}) async-start(bf16[8,4,32,512]{3,2,1,0:T(8,128)(2,1)} %stack.26), calls=%async_computation.9 | async-start | bytes 2097152 | tf_op jit(solution)/shard_map/all_to_all | solution.py:69
  96.5 22.5 %all-to-all-done.9 = bf16[8,4,32,512]{3,2,1,0:T(8,128)(2,1)S(1)} async-done(((bf16[8,4,32,512]{3,2,1,0:T(8,128)(2,1)}), bf16[8,4,32,512]{3,2,1,0:T(8,128)(2,1)S(1)}, u32[]{:S(2)}, u32[]{:S(2)}) %all-to-all-start.9) | async-done | bytes 1048608 | tf_op jit(solution)/shard_map/all_to_all | solution.py:69
  118.9 3.5 %all-to-all-start.3 = ((bf16[4,64,4,512]{3,1,2,0:T(8,128)(2,1)}), bf16[4,64,4,512]{3,1,2,0:T(8,128)(2,1)S(1)}, u32[]{:S(2)}, u32[]{:S(2)}) async-start(bf16[4,64,4,512]{3,1,2,0:T(8,128)(2,1)} %bitcast.79), calls=%async_computation.3 | async-start | bytes 2097152 | tf_op jit(solution)/shard_map/all_to_all | solution.py:30
  127.9 7.2 %all-to-all-done.3 = bf16[4,64,4,512]{3,1,2,0:T(8,128)(2,1)S(1)} async-done(((bf16[4,64,4,512]{3,1,2,0:T(8,128)(2,1)}), bf16[4,64,4,512]{3,1,2,0:T(8,128)(2,1)S(1)}, u32[]{:S(2)}, u32[]{:S(2)}) %all-to-all-start.3) | async-done | bytes 1048608 | tf_op jit(solution)/shard_map/all_to_all | solution.py:30
  135.7 3.9 %all_to_all.63 = bf16[32,2,1,4,512]{4,3,0,2,1:T(4,128)(2,1)S(1)} all-to-all(bf16[32,2,1,4,512]{4,3,0,2,1:T(4,128)(2,1)S(1)} %copy.74), channel_id=1, replica_groups=mesh['ep_0'=8,'ep_1'=4,'ep_2'=2,'tp'=4] {'ep_2'}, dimensions={1} | all-to-all | bytes 524288 | tf_op jit(solution)/shard_map/all_to_all | solution.py:44
  139.6 3.8 %all-to-all-start.10 = ((bf16[2,32,32,512]{3,2,1,0:T(8,128)(2,1)}), bf16[2,32,32,512]{3,2,1,0:T(8,128)(2,1)S(1)}, u32[]{:S(2)}, u32[]{:S(2)}) async-start(bf16[2,32,32,512]{3,2,1,0:T(8,128)(2,1)} %pad_maximum_fusion), calls=%async_computation.10 | async-start | bytes 4194304 | tf_op jit(solution)/shard_map/all_to_all | solution.py:69
  144.2 2.1 all-to-all-done.10
  146.3 7.8 %all-to-all-start.5 = ((bf16[32,2,1,4,512]{4,3,1,2,0:T(4,128)(2,1)}), bf16[32,2,1,4,512]{4,3,1,2,0:T(4,128)(2,1)S(1)}, u32[]{:S(2)}, u32[]{:S(2)}) async-start(bf16[32,2,1,4,512]{4,3,1,2,0:T(4,128)(2,1)} %copy.75), calls=%async_computation.5 | async-start | bytes 524288 | tf_op jit(solution)/shard_map/all_to_all | solution.py:44
  156.3 3.0 %convolution_convert_fusion.1 = bf16[32,2048]{1,0:T(8,128)(2,1)} fusion(bf16[32,512]{1,0:T(8,128)(2,1)} %copy-done.7, bf16[2048,1024]{1,0:T(8,128)(2,1)} %all-gather.2.cloned.1.call-done), kind=kOutput, calls=%fused_computation.3 | convolution fusion | flops 67174400 | bytes 2260992 | tf_op jit(solution)/shard_map/sd,cd->sc/dot_general | solution.py:212
  159.3 7.7 %all-to-all-done.5 = bf16[32,2,1,4,512]{4,3,1,2,0:T(4,128)(2,1)S(1)} async-done(((bf16[32,2,1,4,512]{4,3,1,2,0:T(4,128)(2,1)}), bf16[32,2,1,4,512]{4,3,1,2,0:T(4,128)(2,1)S(1)}, u32[]{:S(2)}, u32[]{:S(2)}) %all-to-all-start.5) | async-done | bytes 262176 | tf_op jit(solution)/shard_map/all_to_all | solution.py:44
  168.8 4.1 %all-to-all-start.7 = ((bf16[4,32,2048]{2,1,0:T(8,128)(2,1)}), bf16[4,32,2048]{2,1,0:T(8,128)(2,1)}, u32[]{:S(2)}, u32[]{:S(2)}) async-start(bf16[4,32,2048]{2,1,0:T(8,128)(2,1)} %broadcast_in_dim.34), calls=%async_computation.7 | async-start | bytes 1048576 | tf_op jit(solution)/shard_map/all_to_all | solution.py:13
  174.3 3.0 %convolution_convert_fusion.2 = bf16[32,2048]{1,0:T(8,128)(2,1)} fusion(bf16[32,512]{1,0:T(8,128)(2,1)} %copy-done.7, bf16[2048,1024]{1,0:T(8,128)(2,1)} %all-gather.2.cloned.1.call-done), kind=kOutput, calls=%fused_computation.4 | convolution fusion | flops 67174400 | bytes 2260992 | tf_op jit(solution)/shard_map/sd,cd->sc/dot_general | solution.py:209
  177.3 4.0 %all-to-all-done.7 = bf16[4,32,2048]{2,1,0:T(8,128)(2,1)} async-done(((bf16[4,32,2048]{2,1,0:T(8,128)(2,1)}), bf16[4,32,2048]{2,1,0:T(8,128)(2,1)}, u32[]{:S(2)}, u32[]{:S(2)}) %all-to-all-start.7) | async-done | bytes 524320 | tf_op jit(solution)/shard_map/all_to_all | solution.py:13
  183.1 4.1 %all-to-all-start.6 = ((bf16[4,32,2048]{2,1,0:T(8,128)(2,1)}), bf16[4,32,2048]{2,1,0:T(8,128)(2,1)}, u32[]{:S(2)}, u32[]{:S(2)}) async-start(bf16[4,32,2048]{2,1,0:T(8,128)(2,1)} %broadcast_in_dim.33), calls=%async_computation.6 | async-start | bytes 1048576 | tf_op jit(solution)/shard_map/all_to_all | solution.py:13
  196.5 2.0 multiply_reduce_fusion.4
  199.1 3.8 %all-to-all-start.11 = ((f32[4,1,32]{2,1,0:T(1,128)}), f32[4,1,32]{2,1,0:T(1,128)S(1)}, u32[]{:S(2)}, u32[]{:S(2)}) async-start(f32[4,1,32]{2,1,0:T(1,128)} %broadcast_in_dim.35), calls=%async_computation.11 | async-start | bytes 4096 | tf_op jit(solution)/shard_map/all_to_all | solution.py:13
  203.5 4.6 %all-to-all-done.11 = f32[4,1,32]{2,1,0:T(1,128)S(1)} async-done(((f32[4,1,32]{2,1,0:T(1,128)}), f32[4,1,32]{2,1,0:T(1,128)S(1)}, u32[]{:S(2)}, u32[]{:S(2)}) %all-to-all-start.11) | async-done | bytes 544 | tf_op jit(solution)/shard_map/all_to_all | solution.py:13
  (139 shorter events, 47.4 us)
Async XLA Ops:
  7.2 87.7 %copy-start = (bf16[1,256,2048]{2,1,0:T(8,128)(2,1)S(1)}, bf16[1,256,2048]{2,1,0:T(8,128)(2,1)}, u32[]{:S(2)}) copy-start(bf16[1,256,2048]{2,1,0:T(8,128)(2,1)} %param.48) | copy-start | bytes 3145732
  7.2 8.5 %copy-start.2 = (bf16[32,2048]{1,0:T(8,128)(2,1)S(1)}, bf16[32,2048]{1,0:T(8,128)(2,1)}, u32[]{:S(2)}) copy-start(bf16[32,2048]{1,0:T(8,128)(2,1)} %param.27) | copy-start | bytes 393220
  7.2 7.6 %copy-start.10 = (bf16[32,3,3,128]{3,0,2,1:T(8,128)(2,1)S(1)}, bf16[32,3,3,128]{3,0,2,1:T(8,128)(2,1)}, u32[]{:S(2)}) copy-start(bf16[32,3,3,128]{3,0,2,1:T(8,128)(2,1)} %param.37) | copy-start | bytes 221188
  7.2 8.4 %copy-start.23 = (f32[2]{0:T(128)S(1)}, f32[2]{0:T(128)}, u32[]{:S(2)}) copy-start(f32[2]{0:T(128)} %param.35) | copy-start | bytes 28
  7.2 8.4 %copy-start.22 = (bf16[2048,8]{0,1:T(8,128)(2,1)S(1)}, bf16[2048,8]{0,1:T(8,128)(2,1)}, u32[]{:S(2)}) copy-start(bf16[2048,8]{0,1:T(8,128)(2,1)} %param.33) | copy-start | bytes 98308
  7.2 8.6 %copy-start.20 = (f32[2]{0:T(128)S(1)}, f32[2]{0:T(128)}, u32[]{:S(2)}) copy-start(f32[2]{0:T(128)} %param.34) | copy-start | bytes 28
  7.2 9.0 %copy-start.3 = (f32[32,2,64,128]{3,2,1,0:T(8,128)S(1)}, f32[32,2,64,128]{3,2,1,0:T(8,128)}, u32[]{:S(2)}) copy-start(f32[32,2,64,128]{3,2,1,0:T(8,128)} %param.38) | copy-start | bytes 6291460
  7.3 149.0 %all-gather.2.cloned.1.call-start = ((), (), s32[]{:S(2)}) async-start(), calls=%async_computation.12 | async-start | bytes 4259840 | tf_op jit(solution)/shard_map/all_gather | solution.py:61
  18.4 16.4 %copy-start.11 = (bf16[32,512]{1,0:T(8,128)(2,1)S(1)}, bf16[32,512]{1,0:T(8,128)(2,1)}, u32[]{:S(2)}) copy-start(bf16[32,512]{1,0:T(8,128)(2,1)} %param.52) | copy-start | bytes 98308
  21.1 13.8 %all-to-all-start = ((bf16[4,32,2048]{2,1,0:T(8,128)(2,1)}), bf16[4,32,2048]{2,1,0:T(8,128)(2,1)S(1)}, u32[]{:S(2)}, u32[]{:S(2)}) async-start(bf16[4,32,2048]{2,1,0:T(8,128)(2,1)} %broadcast_in_dim.23), calls=%async_computation | async-start | bytes 1048576 | tf_op jit(solution)/shard_map/all_to_all | solution.py:13
  35.5 10.4 %all-to-all-start.8 = ((bf16[4,1,32,512]{3,2,1,0:T(8,128)(2,1)}), bf16[4,1,32,512]{3,2,1,0:T(8,128)(2,1)S(1)}, u32[]{:S(2)}, u32[]{:S(2)}) async-start(bf16[4,1,32,512]{3,2,1,0:T(8,128)(2,1)} %stack.25), calls=%async_computation.8 | async-start | bytes 262144 | tf_op jit(solution)/shard_map/all_to_all | solution.py:69
  87.5 31.4 %all-to-all-start.9 = ((bf16[8,4,32,512]{3,2,1,0:T(8,128)(2,1)}), bf16[8,4,32,512]{3,2,1,0:T(8,128)(2,1)S(1)}, u32[]{:S(2)}, u32[]{:S(2)}) async-start(bf16[8,4,32,512]{3,2,1,0:T(8,128)(2,1)} %stack.26), calls=%async_computation.9 | async-start | bytes 2097152 | tf_op jit(solution)/shard_map/all_to_all | solution.py:69
  95.3 27.7 %copy-start.17 = (bf16[2048]{0:T(1024)(128)(2,1)S(1)}, bf16[2048]{0:T(1024)(128)(2,1)}, u32[]{:S(2)}) copy-start(bf16[2048]{0:T(1024)(128)(2,1)} %param.49) | copy-start | bytes 12292
  95.4 30.8 %copy-start.9 = (bf16[2048,64]{0,1:T(8,128)(2,1)S(1)}, bf16[2048,64]{0,1:T(8,128)(2,1)}, u32[]{:S(2)}) copy-start(bf16[2048,64]{0,1:T(8,128)(2,1)} %param.44) | copy-start | bytes 786436
  118.9 16.2 %all-to-all-start.3 = ((bf16[4,64,4,512]{3,1,2,0:T(8,128)(2,1)}), bf16[4,64,4,512]{3,1,2,0:T(8,128)(2,1)S(1)}, u32[]{:S(2)}, u32[]{:S(2)}) async-start(bf16[4,64,4,512]{3,1,2,0:T(8,128)(2,1)} %bitcast.79), calls=%async_computation.3 | async-start | bytes 2097152 | tf_op jit(solution)/shard_map/all_to_all | solution.py:30
  139.6 6.6 %all-to-all-start.10 = ((bf16[2,32,32,512]{3,2,1,0:T(8,128)(2,1)}), bf16[2,32,32,512]{3,2,1,0:T(8,128)(2,1)S(1)}, u32[]{:S(2)}, u32[]{:S(2)}) async-start(bf16[2,32,32,512]{3,2,1,0:T(8,128)(2,1)} %pad_maximum_fusion), calls=%async_computation.10 | async-start | bytes 4194304 | tf_op jit(solution)/shard_map/all_to_all | solution.py:69
  146.3 20.7 %all-to-all-start.5 = ((bf16[32,2,1,4,512]{4,3,1,2,0:T(4,128)(2,1)}), bf16[32,2,1,4,512]{4,3,1,2,0:T(4,128)(2,1)S(1)}, u32[]{:S(2)}, u32[]{:S(2)}) async-start(bf16[32,2,1,4,512]{4,3,1,2,0:T(4,128)(2,1)} %copy.75), calls=%async_computation.5 | async-start | bytes 524288 | tf_op jit(solution)/shard_map/all_to_all | solution.py:44
  155.6 17.4 %copy-start.14 = (f32[32,4]{0,1:T(4,128)S(1)}, f32[32,4]{0,1:T(4,128)}, u32[]{:S(2)}) copy-start(f32[32,4]{0,1:T(4,128)} %copy-done.13) | copy-start | bytes 1540
  166.9 16.1 %copy-start.5 = (bf16[32,2,1,4,512]{4,3,1,2,0:T(4,128)(2,1)}, bf16[32,2,1,4,512]{4,3,1,2,0:T(4,128)(2,1)S(1)}, u32[]{:S(2)}) copy-start(bf16[32,2,1,4,512]{4,3,1,2,0:T(4,128)(2,1)S(1)} %all-to-all-done.5) | copy-start | bytes 786436
  168.8 12.5 %all-to-all-start.7 = ((bf16[4,32,2048]{2,1,0:T(8,128)(2,1)}), bf16[4,32,2048]{2,1,0:T(8,128)(2,1)}, u32[]{:S(2)}, u32[]{:S(2)}) async-start(bf16[4,32,2048]{2,1,0:T(8,128)(2,1)} %broadcast_in_dim.34), calls=%async_computation.7 | async-start | bytes 1048576 | tf_op jit(solution)/shard_map/all_to_all | solution.py:13
  183.1 12.3 %all-to-all-start.6 = ((bf16[4,32,2048]{2,1,0:T(8,128)(2,1)}), bf16[4,32,2048]{2,1,0:T(8,128)(2,1)}, u32[]{:S(2)}, u32[]{:S(2)}) async-start(bf16[4,32,2048]{2,1,0:T(8,128)(2,1)} %broadcast_in_dim.33), calls=%async_computation.6 | async-start | bytes 1048576 | tf_op jit(solution)/shard_map/all_to_all | solution.py:13
  193.2 9.7 %copy-start.19 = (bf16[512]{0:T(512)(128)(2,1)S(1)}, bf16[512]{0:T(512)(128)(2,1)}, u32[]{:S(2)}) copy-start(bf16[512]{0:T(512)(128)(2,1)} %param.53) | copy-start | bytes 3076
  193.2 9.7 %copy-start.8 = (bf16[32,3,4,128]{3,0,2,1:T(8,128)(2,1)S(1)}, bf16[32,3,4,128]{3,0,2,1:T(8,128)(2,1)}, u32[]{:S(2)}) copy-start(bf16[32,3,4,128]{3,0,2,1:T(8,128)(2,1)} %get-tuple-element.10) | copy-start | bytes 294916
  199.1 9.0 %all-to-all-start.11 = ((f32[4,1,32]{2,1,0:T(1,128)}), f32[4,1,32]{2,1,0:T(1,128)S(1)}, u32[]{:S(2)}, u32[]{:S(2)}) async-start(f32[4,1,32]{2,1,0:T(1,128)} %broadcast_in_dim.35), calls=%async_computation.11 | async-start | bytes 4096 | tf_op jit(solution)/shard_map/all_to_all | solution.py:13
  (11 other events, 42.6 us)
Sparse Core Ops, SparseCore 0:
  11.4 80.8 all-gather.1
